TPU v7x, 32 devices: a whole 2x2x4 slice. The times are simulated.
32 devices in a mesh: sp: 8 (over z, x), tp: 4 (over y, core).
Axes of the slice: x: 2, y: 2, z: 4, core: 2. Of those that a mesh axis runs over, the one named last changes fastest.
Arguments:
- skip_stream_input: bfloat16 [1024, 2048], P('sp'), may hold values from -16 to 16
- asking_vectors_split: bfloat16 [1024, 2048], P('sp', 'tp'), may hold values from -8 to 8
- lookup_vectors_split: bfloat16 [1024, 512], P('sp'), may hold values from -8 to 8
- content_vectors_split: bfloat16 [1024, 512], P('sp'), may hold values from -6 to 6
- asking_rms_gain: float32 [128], replicated, may hold values from 0.1 to 1.9
- lookup_rms_gain: float32 [128], replicated, may hold values from 0.1 to 1.9
- softness_per_channel: float32 [16], P('tp'), may hold values from 1.5 to 24
- mixing_exit_weights: bfloat16 [2048, 2048], P('tp'), may hold values from -0.125 to 0.125
- specialist_rms_gain: float32 [2048], replicated, may hold values from 0.1 to 1.9
- selected_dispatch_weights: float32 [1024, 2], P('sp'), may hold values from -6 to 6
- selected_specialist_ids: int32 [1024, 2], P('sp'), may hold values from 0 to 7, all different within a row; in each aligned block of 128 rows (0 to 127, 128 to 255, ...) at most 48 rows name the same one
- specialist_switch_weights: bfloat16 [8, 2048, 2048], P('sp', None, 'tp'), may hold values from -0.125 to 0.125
- specialist_widen_weights: bfloat16 [8, 2048, 2048], P('sp', None, 'tp'), may hold values from -0.125 to 0.125
- specialist_shrink_weights: bfloat16 [8, 2048, 2048], P('sp', 'tp'), may hold values from -0.125 to 0.125
Outputs:
- layer_out: bfloat16 [1024, 2048], P('sp', 'tp')
Inputs may be any that keep to these rules, and one draw needn't show every extreme that they name: `selected_specialist_ids`: each row names 2 different experts. In each aligned block of 128 rows no expert is named by more than 48 rows, a bound that some block reaches.
All inputs are finite; a program needn't handle non-finite values.
Results may differ from a plain program's by a relative error of at most 0.0085.
Values may be sent and summed in bfloat16 or wider, within the bound.
A program may use at most 64 MiB of HBM per device.

v0:
```python
import math
import jax
import jax.numpy as jnp
from jax import lax
from jax.sharding import PartitionSpec as P

CHANNEL_WIDTH = 128
GROUP = 4
GRID_W = 64
EPSILON = 1e-06
NEGATIVE = -1e30


def rotate_half(values_in, positions, full_width):
    half_width = full_width // 2
    frequency = 10000.0 ** (-jnp.arange(half_width, dtype=jnp.float32) / half_width)
    angles = positions.astype(jnp.float32)[:, None] * frequency[None, :]
    cosine = jnp.cos(angles)[:, None, :]
    sine = jnp.sin(angles)[:, None, :]
    leading = values_in[..., :half_width]
    trailing = values_in[..., half_width:]
    return jnp.concatenate(
        [leading * cosine - trailing * sine, trailing * cosine + leading * sine], axis=-1
    )


def norm_rotate(heads_in, gain_vec, positions):
    widened = heads_in.astype(jnp.float32)
    scaled = (
        widened
        * lax.rsqrt(jnp.mean(widened * widened, axis=-1, keepdims=True) + EPSILON)
        * gain_vec
    )
    half_width = scaled.shape[-1] // 2
    grid_rows = positions // GRID_W
    grid_cols = positions % GRID_W
    turned = jnp.concatenate(
        [
            rotate_half(scaled[..., :half_width], grid_rows, half_width),
            rotate_half(scaled[..., half_width:], grid_cols, half_width),
        ],
        axis=-1,
    )
    return turned.astype(jnp.bfloat16)


def shards(
    skip_stream_input,
    asking_vectors_split,
    lookup_vectors_split,
    content_vectors_split,
    asking_rms_gain,
    lookup_rms_gain,
    softness_per_channel,
    mixing_exit_weights,
    specialist_rms_gain,
    selected_dispatch_weights,
    selected_specialist_ids,
    specialist_switch_weights,
    specialist_widen_weights,
    specialist_shrink_weights,
):
    tok_count = skip_stream_input.shape[0]
    model_width = skip_stream_input.shape[1]
    heads_here = asking_vectors_split.shape[1] // CHANNEL_WIDTH
    local_key_value_heads = max(1, heads_here // GROUP)
    local_group_count = heads_here // local_key_value_heads
    tp_position = lax.axis_index("tp")
    positions = lax.axis_index("sp") * tok_count + jnp.arange(tok_count, dtype=jnp.int32)
    query_turned = norm_rotate(
        asking_vectors_split.reshape(tok_count, heads_here, CHANNEL_WIDTH),
        asking_rms_gain,
        positions,
    )
    first_head = tp_position * heads_here // GROUP
    key_cols = lax.dynamic_slice_in_dim(
        lookup_vectors_split, first_head * CHANNEL_WIDTH, local_key_value_heads * CHANNEL_WIDTH, 1
    )
    value_cols = lax.dynamic_slice_in_dim(
        content_vectors_split, first_head * CHANNEL_WIDTH, local_key_value_heads * CHANNEL_WIDTH, 1
    )
    key_turned = norm_rotate(
        key_cols.reshape(tok_count, local_key_value_heads, CHANNEL_WIDTH),
        lookup_rms_gain,
        positions,
    )
    key_turned = key_turned.reshape(tok_count, local_key_value_heads * CHANNEL_WIDTH)
    query_grouped = query_turned.reshape(
        tok_count, local_key_value_heads, local_group_count, CHANNEL_WIDTH
    ).transpose(1, 2, 0, 3)
    inverse_root_width = (softness_per_channel / math.sqrt(CHANNEL_WIDTH)).reshape(
        local_key_value_heads, local_group_count, 1, 1
    )

    def absorb(run_state, key_span, value_span):
        run_max, run_sum, run_acc = run_state
        scores = (
            jnp.einsum(
                "kgqd,nkd->kgqn", query_grouped, key_span, preferred_element_type=jnp.float32
            )
            * inverse_root_width
        )
        new_max = jnp.maximum(run_max, jnp.max(scores, axis=-1))
        factor = jnp.exp(run_max - new_max)
        exp_terms = jnp.exp(scores - new_max[..., None])
        run_sum = run_sum * factor + jnp.sum(exp_terms, axis=-1)
        run_acc = run_acc * factor[..., None] + jnp.einsum(
            "kgqn,nkd->kgqd",
            exp_terms.astype(jnp.bfloat16),
            value_span,
            preferred_element_type=jnp.float32,
        )
        return (new_max, run_sum, run_acc)

    initial = (
        jnp.full((local_key_value_heads, local_group_count, tok_count), NEGATIVE, jnp.float32),
        jnp.zeros((local_key_value_heads, local_group_count, tok_count), jnp.float32),
        jnp.zeros(
            (local_key_value_heads, local_group_count, tok_count, CHANNEL_WIDTH), jnp.float32
        ),
    )
    key_piece = lax.all_gather(key_turned, "sp", axis=0, tiled=True)
    value_piece = lax.all_gather(value_cols, "sp", axis=0, tiled=True)
    piece_len = key_piece.shape[0]
    span_len = 1024
    span_count = piece_len // span_len
    key_spans = key_piece.reshape(span_count, span_len, local_key_value_heads, CHANNEL_WIDTH)
    value_spans = value_piece.reshape(span_count, span_len, local_key_value_heads, CHANNEL_WIDTH)

    def step_span(inner_state, span_pair):
        return (absorb(inner_state, span_pair[0], span_pair[1]), None)

    result_state, unused = lax.scan(step_span, initial, (key_spans, value_spans))
    final_max, final_sum, final_acc = result_state
    attn_heads = (final_acc / final_sum[..., None]).astype(jnp.bfloat16)
    attn_flat = attn_heads.transpose(2, 0, 1, 3).reshape(tok_count, heads_here * CHANNEL_WIDTH)
    partial_sum = jnp.dot(attn_flat, mixing_exit_weights, preferred_element_type=jnp.float32)
    share_width = model_width // lax.axis_size("tp")
    first_col = tp_position * share_width
    attended = lax.psum(partial_sum.astype(jnp.bfloat16), "tp")
    mid_rows = (skip_stream_input.astype(jnp.float32) + attended.astype(jnp.float32)).astype(
        jnp.bfloat16
    )
    mid_wide = mid_rows.astype(jnp.float32)
    normed_rows = (
        mid_wide
        * lax.rsqrt(jnp.mean(mid_wide * mid_wide, axis=-1, keepdims=True) + EPSILON)
        * specialist_rms_gain
    ).astype(jnp.bfloat16)
    mid_share = lax.dynamic_slice_in_dim(mid_rows, first_col, share_width, 1)
    outgoing_rows = lax.dynamic_slice_in_dim(normed_rows, first_col, share_width, 1)
    experts_count = lax.axis_size("sp")
    top_count = selected_specialist_ids.shape[1]
    capacity = max(2, 3 * tok_count * top_count // (2 * experts_count))
    flat_ids = selected_specialist_ids.reshape(-1)
    one_hot = (flat_ids[:, None] == jnp.arange(experts_count, dtype=jnp.int32)[None, :]).astype(
        jnp.int32
    )
    earlier = jnp.cumsum(one_hot, axis=0) - one_hot
    slot_index = jnp.sum(earlier * one_hot, axis=1)
    destination = flat_ids * capacity + slot_index
    owner_rows = jnp.arange(tok_count * top_count, dtype=jnp.int32) // top_count
    slot_owner = jnp.zeros((experts_count * capacity,), jnp.int32).at[destination].set(owner_rows)
    filled = jnp.zeros((experts_count * capacity,), jnp.int32).at[destination].set(1)
    outgoing = jnp.where(
        filled[:, None] > 0, outgoing_rows[slot_owner], jnp.zeros((), jnp.bfloat16)
    )
    outgoing = outgoing.reshape(experts_count, capacity, outgoing_rows.shape[1])
    gate_local = specialist_switch_weights[0]
    up_local = specialist_widen_weights[0]
    down_local = specialist_shrink_weights[0]
    arrived = lax.all_to_all(outgoing, "sp", split_axis=0, concat_axis=0, tiled=True)
    row_count = arrived.shape[0] * arrived.shape[1]
    feature_piece = lax.all_gather(arrived, "tp", axis=2, tiled=True)
    piece_width = feature_piece.shape[2]
    flat_piece = feature_piece.reshape(row_count, piece_width)
    gate_acc = jnp.dot(flat_piece, gate_local, preferred_element_type=jnp.float32)
    up_acc = jnp.dot(flat_piece, up_local, preferred_element_type=jnp.float32)
    hidden = (jax.nn.silu(gate_acc) * up_acc).astype(jnp.bfloat16)
    expert_part = jnp.dot(hidden, down_local, preferred_element_type=jnp.float32)
    expert_part = expert_part.reshape(arrived.shape[0], arrived.shape[1], model_width)
    expert_share = lax.psum_scatter(
        expert_part.astype(jnp.bfloat16), "tp", scatter_dimension=2, tiled=True
    )
    returned = lax.all_to_all(expert_share, "sp", split_axis=0, concat_axis=0, tiled=True)
    back_flat = returned.reshape(experts_count * capacity, share_width)
    picked = back_flat[destination].reshape(tok_count, top_count, share_width).astype(jnp.float32)
    route_weights = jax.nn.softmax(selected_dispatch_weights, axis=-1)
    layer_out = mid_share.astype(jnp.float32) + jnp.sum(route_weights[..., None] * picked, axis=1)
    return layer_out.astype(jnp.bfloat16)


def solution(mesh):
    in_specs = (
        P("sp", None),
        P("sp", "tp"),
        P("sp", None),
        P("sp", None),
        P(),
        P(),
        P("tp"),
        P("tp", None),
        P(),
        P("sp", None),
        P("sp", None),
        P("sp", None, "tp"),
        P("sp", None, "tp"),
        P("sp", "tp", None),
    )
    out_specs = P("sp", "tp")
    return jax.shard_map(shards, mesh=mesh, in_specs=in_specs, out_specs=out_specs, check_vma=False)
```

profile of v0, /device:TPU:0, one launch (start us, length us, event | category | flops | bytes accessed | tf_op | source)
XLA Modules:
  0.0 204.7 jit_solution(4723165117829957611)
XLA Ops:
  6.6 0.9 constant_dynamic-slice_fusion.1
  9.2 28.3 %all_gather.9 = bf16[1024,128]{0,1:T(8,128)(2,1)S(1)} all-gather(bf16[128,128]{0,1:T(8,128)(2,1)S(1)} %pad_maximum_fusion), channel_id=1, replica_groups=mesh['sp'=8,'tp'=4] {'sp'}, dimensions={0}, use_global_device_ids=true | all-gather | bytes 294912 | tf_op jit(solution)/shard_map/all_gather | solution.py:122
  37.5 1.0 copy.24
  39.4 0.8 multiply_multiply_fusion
  41.1 1.3 copy-done.1
  42.9 0.8 constant_dynamic-slice_fusion
  43.8 26.8 %all_gather.10 = bf16[1024,128]{0,1:T(8,128)(2,1)S(1)} all-gather(bf16[128,128]{0,1:T(8,128)(2,1)S(1)} %copy.36), channel_id=1, replica_groups=mesh['sp'=8,'tp'=4] {'sp'}, dimensions={0}, use_global_device_ids=true | all-gather | bytes 294912 | tf_op jit(solution)/shard_map/all_gather | solution.py:123
  70.7 2.2 %fusion.14 = bf16[4,128,128]{1,2,0:T(8,128)(2,1)S(1)} fusion(f32[4,128,1024]{2,1,0:T(8,128)} %copy-done.1, f32[4,128]{1,0:T(4,128)S(1)} %broadcast_maximum_fusion, f32[4]{0:T(128)S(1)} %broadcast_multiply_fusion.1, bf16[1024,128]{0,1:T(8,128)(2,1)S(1)} %all_gather.10, f32[4,128]{1,0:T(4,128)S(1)} %get-tuple-element.44, f32[4,128]{1,0:T(4,128)S(1)} %get-tuple-element.43), kind=kOutput, calls=%fused_computation.19 | convolution fusion | flops 135987200 | bytes 2496528 | tf_op jit(solution)/shard_map/while/body/eval_jaxpr/kgqn,nkd->kgqd/dot_general | solution.py:107
  72.9 1.3 convolution_convert_fusion.1
  75.9 1.4 scatter_custom_fusion.1
  77.3 1.4 scatter_custom_fusion
  78.8 0.8 dynamic-slice
  79.6 25.8 %all-reduce.2.cloned.1.call-done = bf16[128,2048]{1,0:T(8,128)(2,1)} async-done(((bf16[128,2048]{1,0:T(8,128)(2,1)}), bf16[128,2048]{1,0:T(8,128)(2,1)}) %all-reduce.2.cloned.1.call-update) | async-done | bytes 524304 | tf_op jit(solution)/shard_map/psum | solution.py:140
  105.4 1.3 multiply_reduce_fusion.1
  106.9 2.1 %gather_fusion = bf16[384,512]{1,0:T(8,128)(2,1)S(1)} fusion(bf16[128,512]{1,0:T(8,128)(2,1)S(1)} %fusion.19, s32[1024]{0:T(1024)S(1)} %pad_clamp_fusion.1), kind=kCustom, calls=%fused_computation | custom fusion | bytes 787968 | tf_op jit(solution)/shard_map/gather | solution.py:166
  109.1 16.5 %all_to_all.10 = bf16[8,48,512]{2,1,0:T(8,128)(2,1)} all-to-all(bf16[8,48,512]{2,1,0:T(8,128)(2,1)S(1)} %broadcast_select_fusion), channel_id=1, replica_groups=mesh['sp'=8,'tp'=4] {'sp'}, dimensions={0} | all-to-all | bytes 786432 | tf_op jit(solution)/shard_map/all_to_all | solution.py:172
  125.7 18.0 %all-gather.2.cloned.1.call-done = bf16[8,48,2048]{2,1,0:T(8,128)(2,1)} async-done(((bf16[8,48,512]{2,1,0:T(8,128)(2,1)}), bf16[8,48,2048]{2,1,0:T(8,128)(2,1)}) %all-gather.2.cloned.1.call-update) | async-done | bytes 1572880 | tf_op jit(solution)/shard_map/all_gather | solution.py:174
  143.7 3.2 %fusion.3 = f32[384,512]{1,0:T(8,128)S(1)} fusion(bf16[384,2048]{1,0:T(8,128)(2,1)} %bitcast.82, bf16[1,2048,512]{2,1,0:T(8,128)(2,1)} %param.25), kind=kOutput, calls=%fused_computation.9 | convolution fusion | flops 805306368 | bytes 4456448 | tf_op jit(solution)/shard_map/dot_general | solution.py:177
  146.9 1.0 fusion.10
  147.9 2.1 %convolution_convert_fusion = bf16[8,48,2048]{2,1,0:T(8,128)(2,1)} fusion(bf16[8,48,512]{2,1,0:T(8,128)(2,1)S(1)} %bitcast.84, bf16[1,512,2048]{2,1,0:T(8,128)(2,1)S(1)} %copy-done), kind=kOutput, calls=%fused_computation.4 | convolution fusion | flops 806092800 | bytes 4063232 | tf_op jit(solution)/shard_map/dot_general | solution.py:180
  150.1 28.1 %reduce-scatter.2.cloned.1.call-done = bf16[8,48,512]{2,1,0:T(8,128)(2,1)} async-done(((bf16[8,48,2048]{2,1,0:T(8,128)(2,1)}), bf16[8,48,512]{2,1,0:T(8,128)(2,1)}) %reduce-scatter.2.cloned.1.call-update) | async-done | bytes 393232 | tf_op jit(solution)/shard_map/reduce_scatter | solution.py:182
  178.2 5.5 %all-to-all-start.1 = ((bf16[8,48,512]{2,1,0:T(8,128)(2,1)}), bf16[8,48,512]{2,1,0:T(8,128)(2,1)S(1)}, u32[]{:S(2)}, u32[]{:S(2)}) async-start(bf16[8,48,512]{2,1,0:T(8,128)(2,1)} %reduce-scatter.2.cloned.1.call-done), calls=%async_computation.2 | async-start | bytes 786432 | tf_op jit(solution)/shard_map/all_to_all | solution.py:185
  183.9 11.4 %all-to-all-done.1 = bf16[8,48,512]{2,1,0:T(8,128)(2,1)S(1)} async-done(((bf16[8,48,512]{2,1,0:T(8,128)(2,1)}), bf16[8,48,512]{2,1,0:T(8,128)(2,1)S(1)}, u32[]{:S(2)}, u32[]{:S(2)}) %all-to-all-start.1) | async-done | bytes 393248 | tf_op jit(solution)/shard_map/all_to_all | solution.py:185
  195.3 1.2 gather_fusion.1
  (71 shorter events, 8.1 us)
Async XLA Ops:
  6.5 141.4 %copy-start = (bf16[1,512,2048]{2,1,0:T(8,128)(2,1)S(1)}, bf16[1,512,2048]{2,1,0:T(8,128)(2,1)}, u32[]{:S(2)}) copy-start(bf16[1,512,2048]{2,1,0:T(8,128)(2,1)} %param.27) | copy-start | bytes 6291460
  6.5 98.8 %all-reduce.2.cloned.1.call-start = ((), (), s32[]{:S(2)}) async-start(), calls=%async_computation.3 | async-start | bytes 1048576 | tf_op jit(solution)/shard_map/psum | solution.py:140
  41.1 1.4 copy-start.1
  43.8 29.1 %copy-start.2 = (bf16[512,2048]{1,0:T(8,128)(2,1)S(1)}, bf16[512,2048]{1,0:T(8,128)(2,1)}, u32[]{:S(2)}) copy-start(bf16[512,2048]{1,0:T(8,128)(2,1)} %param.21) | copy-start | bytes 6291460
  72.9 1.4 copy-start.5
  72.9 32.5 %copy-start.3 = (bf16[128,2048]{1,0:T(8,128)(2,1)S(1)}, bf16[128,2048]{1,0:T(8,128)(2,1)}, u32[]{:S(2)}) copy-start(bf16[128,2048]{1,0:T(8,128)(2,1)} %param.14) | copy-start | bytes 1572868
  74.2 69.4 %all-gather.2.cloned.1.call-start = ((), (), s32[]{:S(2)}) async-start(), calls=%async_computation.4 | async-start | bytes 1966080 | tf_op jit(solution)/shard_map/all_gather | solution.py:174
  125.6 52.6 %reduce-scatter.2.cloned.1.call-start = ((), (), s32[]{:S(2)}) async-start(), calls=%async_computation.5 | async-start | bytes 1966080 | tf_op jit(solution)/shard_map/reduce_scatter | solution.py:182
  143.7 3.2 %copy-start.6 = (bf16[1,2048,512]{2,1,0:T(8,128)(2,1)S(1)}, bf16[1,2048,512]{2,1,0:T(8,128)(2,1)}, u32[]{:S(2)}) copy-start(bf16[1,2048,512]{2,1,0:T(8,128)(2,1)} %param.26) | copy-start | bytes 6291460
  143.7 3.2 %copy-start.7 = (bf16[8,48,2048]{2,1,0:T(8,128)(2,1)S(1)}, bf16[8,48,2048]{2,1,0:T(8,128)(2,1)}, u32[]{:S(2)}) copy-start(bf16[8,48,2048]{2,1,0:T(8,128)(2,1)} %all-gather.2.cloned.1.call-done) | copy-start | bytes 4718596
  150.0 33.7 %copy-start.4 = (f32[128,2]{0,1:T(2,128)S(1)}, f32[128,2]{0,1:T(2,128)}, u32[]{:S(2)}) copy-start(f32[128,2]{0,1:T(2,128)} %param.23) | copy-start | bytes 3076
  178.2 17.1 %all-to-all-start.1 = ((bf16[8,48,512]{2,1,0:T(8,128)(2,1)}), bf16[8,48,512]{2,1,0:T(8,128)(2,1)S(1)}, u32[]{:S(2)}, u32[]{:S(2)}) async-start(bf16[8,48,512]{2,1,0:T(8,128)(2,1)} %reduce-scatter.2.cloned.1.call-done), calls=%async_computation.2 | async-start | bytes 786432 | tf_op jit(solution)/shard_map/all_to_all | solution.py:185
Sparse Core Ops, SparseCore 0:
  74.3 30.9 all-reduce.1
  125.8 17.8 all-gather.1
  150.2 27.9 reduce-scatter.1
where the time goes:
time: 205 us
  waiting for transfers between devices  83.3 us (41%)
  blocking collectives  71.7 us (35%)
  between operations  13.5 us (7%)
  local copies, waits for them, and re-layouts  12.6 us (6%)
  matrix products  10.4 us (5%)
  other arithmetic  7.66 us (4%)
  starting transfers between devices  5.57 us (3%)
    all_gather x1, blocking collectives, shards(): key_piece = lax.all_gather(key_turned, 'sp', axis=0, tiled=True)  28.3 us
    reduce_scatter x1, waiting for transfers between devices, shards(): lax.psum_scatter(expert_part.astype(jnp.bfloat16), 'tp', scatter_dimensio...  28.1 us
    all_gather x1, blocking collectives, shards(): value_piece = lax.all_gather(value_cols, 'sp', axis=0, tiled=True)  26.8 us
    psum x1, waiting for transfers between devices, shards(): attended = lax.psum(partial_sum.astype(jnp.bfloat16), 'tp')  25.8 us
    all_gather x1, waiting for transfers between devices, shards(): feature_piece = lax.all_gather(arrived, 'tp', axis=2, tiled=True)  18 us
    all_to_all x1, blocking collectives, shards(): lax.all_to_all(outgoing, 'sp', split_axis=0, concat_axis=0, tiled=True)  16.5 us
    all_to_all x1, waiting for transfers between devices, shards(): lax.all_to_all(expert_share, 'sp', split_axis=0, concat_axis=0, tiled=True)  11.4 us
    all_to_all x1, starting transfers between devices, shards(): lax.all_to_all(expert_share, 'sp', split_axis=0, concat_axis=0, tiled=True)  5.48 us
  transfers between devices with their start and end apart: 4, of which 4 were waited for; matrix products, arithmetic and copies ran while one was open for 3% of the time, Pallas kernels for 0%

commit v1 on v0

--- a/solution.py
+++ b/solution.py
@@ -137,7 +137,7 @@
     partial_sum = jnp.dot(attn_flat, mixing_exit_weights, preferred_element_type=jnp.float32)
     share_width = model_width // lax.axis_size("tp")
     first_col = tp_position * share_width
-    attended = lax.psum(partial_sum.astype(jnp.bfloat16), "tp")
+    attended = jnp.sum(lax.all_gather(partial_sum.astype(jnp.bfloat16), "tp"), axis=0)
     mid_rows = (skip_stream_input.astype(jnp.float32) + attended.astype(jnp.float32)).astype(
         jnp.bfloat16
     )

time: 205 us -> 197 us (0.961)
  waiting for transfers between devices: 83.3 us -> 72 us
    psum x1 -> x0, waiting for transfers between devices: 25.8 us -> none  [shards(): attended = lax.psum(partial_sum.astype(jnp.bfloat16), 'tp')]
    all_gather x0 -> x1, waiting for transfers between devices: none -> 14.9 us  [shards(): lax.all_gather(partial_sum.astype(jnp.bfloat16), 'tp')]
where the time goes in v1:
time: 197 us
  blocking collectives  73 us (37%)
  waiting for transfers between devices  72 us (37%)
  between operations  13.4 us (7%)
  local copies, waits for them, and re-layouts  12.6 us (6%)
  matrix products  10.4 us (5%)
  other arithmetic  9.69 us (5%)
  starting transfers between devices  5.57 us (3%)
    all_gather x1, blocking collectives, shards(): key_piece = lax.all_gather(key_turned, 'sp', axis=0, tiled=True)  28.3 us
    reduce_scatter x1, waiting for transfers between devices, shards(): lax.psum_scatter(expert_part.astype(jnp.bfloat16), 'tp', scatter_dimensio...  28.1 us
    all_gather x1, blocking collectives, shards(): value_piece = lax.all_gather(value_cols, 'sp', axis=0, tiled=True)  26.8 us
    all_to_all x1, blocking collectives, shards(): lax.all_to_all(outgoing, 'sp', split_axis=0, concat_axis=0, tiled=True)  17.9 us
    all_gather x1, waiting for transfers between devices, shards(): feature_piece = lax.all_gather(arrived, 'tp', axis=2, tiled=True)  17.5 us
    all_gather x1, waiting for transfers between devices, shards(): lax.all_gather(partial_sum.astype(jnp.bfloat16), 'tp')  14.9 us
    all_to_all x1, waiting for transfers between devices, shards(): lax.all_to_all(expert_share, 'sp', split_axis=0, concat_axis=0, tiled=True)  11.4 us
    all_to_all x1, starting transfers between devices, shards(): lax.all_to_all(expert_share, 'sp', split_axis=0, concat_axis=0, tiled=True)  5.48 us
  transfers between devices with their start and end apart: 4, of which 4 were waited for; matrix products, arithmetic and copies ran while one was open for 3% of the time, Pallas kernels for 0%

profile of v1, /device:TPU:0, one launch (start us, length us, event | category | flops | bytes accessed | tf_op | source)
XLA Modules:
  0.0 196.7 jit_solution(3682794193251455189)
XLA Ops:
  6.6 0.9 constant_dynamic-slice_fusion.1
  9.2 28.3 %all_gather.15 = bf16[1024,128]{0,1:T(8,128)(2,1)S(1)} all-gather(bf16[128,128]{0,1:T(8,128)(2,1)S(1)} %pad_maximum_fusion), channel_id=1, replica_groups=mesh['sp'=8,'tp'=4] {'sp'}, dimensions={0}, use_global_device_ids=true | all-gather | bytes 294912 | tf_op jit(solution)/shard_map/all_gather | solution.py:122
  37.5 1.0 copy.24
  39.4 0.8 multiply_multiply_fusion
  41.1 1.3 copy-done.1
  42.9 0.8 constant_dynamic-slice_fusion
  43.8 26.8 %all_gather.16 = bf16[1024,128]{0,1:T(8,128)(2,1)S(1)} all-gather(bf16[128,128]{0,1:T(8,128)(2,1)S(1)} %copy.36), channel_id=1, replica_groups=mesh['sp'=8,'tp'=4] {'sp'}, dimensions={0}, use_global_device_ids=true | all-gather | bytes 294912 | tf_op jit(solution)/shard_map/all_gather | solution.py:123
  70.7 2.2 %fusion.14 = bf16[4,128,128]{1,2,0:T(8,128)(2,1)S(1)} fusion(f32[4,128,1024]{2,1,0:T(8,128)} %copy-done.1, f32[4,128]{1,0:T(4,128)S(1)} %broadcast_maximum_fusion, f32[4]{0:T(128)S(1)} %broadcast_multiply_fusion.1, bf16[1024,128]{0,1:T(8,128)(2,1)S(1)} %all_gather.16, f32[4,128]{1,0:T(4,128)S(1)} %get-tuple-element.44, f32[4,128]{1,0:T(4,128)S(1)} %get-tuple-element.43), kind=kOutput, calls=%fused_computation.19 | convolution fusion | flops 135987200 | bytes 2496528 | tf_op jit(solution)/shard_map/while/body/eval_jaxpr/kgqn,nkd->kgqd/dot_general | solution.py:107
  72.9 1.3 convolution_convert_fusion.1
  75.9 1.4 scatter_custom_fusion.1
  77.3 1.4 scatter_custom_fusion
  79.6 14.9 %all-gather.6.cloned.1.call-done = bf16[512,2048]{1,0:T(8,128)(2,1)} async-done(((bf16[128,2048]{1,0:T(8,128)(2,1)}), bf16[512,2048]{1,0:T(8,128)(2,1)}) %all-gather.6.cloned.1.call-update) | async-done | bytes 2097168 | tf_op jit(solution)/shard_map/all_gather | solution.py:140
  94.5 2.0 %reduce_sum.81 = bf16[128,2048]{1,0:T(8,128)(2,1)S(1)} reduce(bf16[4,128,2048]{2,1,0:T(8,128)(2,1)} %bitcast.76, bf16[]{:T(256)} %constant.129.clone.1), dimensions={0}, to_apply=%region_4.5 | reduce | flops 786432 | bytes 2621442 | tf_op jit(solution)/shard_map/reduce_sum | solution.py:140
  96.5 1.3 multiply_reduce_fusion.1
  98.1 2.1 %gather_fusion = bf16[384,512]{1,0:T(8,128)(2,1)S(1)} fusion(bf16[128,512]{1,0:T(8,128)(2,1)S(1)} %fusion.19, s32[1024]{0:T(1024)S(1)} %pad_clamp_fusion.1), kind=kCustom, calls=%fused_computation | custom fusion | bytes 787968 | tf_op jit(solution)/shard_map/gather | solution.py:166
  100.3 17.9 %all_to_all.10 = bf16[8,48,512]{2,1,0:T(8,128)(2,1)} all-to-all(bf16[8,48,512]{2,1,0:T(8,128)(2,1)S(1)} %broadcast_select_fusion), channel_id=1, replica_groups=mesh['sp'=8,'tp'=4] {'sp'}, dimensions={0} | all-to-all | bytes 786432 | tf_op jit(solution)/shard_map/all_to_all | solution.py:172
  118.2 17.5 %all-gather.4.cloned.1.call-done = bf16[8,48,2048]{2,1,0:T(8,128)(2,1)} async-done(((bf16[8,48,512]{2,1,0:T(8,128)(2,1)}), bf16[8,48,2048]{2,1,0:T(8,128)(2,1)}) %all-gather.4.cloned.1.call-update) | async-done | bytes 1572880 | tf_op jit(solution)/shard_map/all_gather | solution.py:174
  135.7 3.2 %fusion.3 = f32[384,512]{1,0:T(8,128)S(1)} fusion(bf16[384,2048]{1,0:T(8,128)(2,1)} %bitcast.84, bf16[1,2048,512]{2,1,0:T(8,128)(2,1)} %param.25), kind=kOutput, calls=%fused_computation.9 | convolution fusion | flops 805306368 | bytes 4456448 | tf_op jit(solution)/shard_map/dot_general | solution.py:177
  138.9 1.0 fusion.10
  139.9 2.1 %convolution_convert_fusion = bf16[8,48,2048]{2,1,0:T(8,128)(2,1)} fusion(bf16[8,48,512]{2,1,0:T(8,128)(2,1)S(1)} %bitcast.86, bf16[1,512,2048]{2,1,0:T(8,128)(2,1)S(1)} %copy-done), kind=kOutput, calls=%fused_computation.4 | convolution fusion | flops 806092800 | bytes 4063232 | tf_op jit(solution)/shard_map/dot_general | solution.py:180
  142.1 28.1 %reduce-scatter.2.cloned.1.call-done = bf16[8,48,512]{2,1,0:T(8,128)(2,1)} async-done(((bf16[8,48,2048]{2,1,0:T(8,128)(2,1)}), bf16[8,48,512]{2,1,0:T(8,128)(2,1)}) %reduce-scatter.2.cloned.1.call-update) | async-done | bytes 393232 | tf_op jit(solution)/shard_map/reduce_scatter | solution.py:182
  170.2 5.5 %all-to-all-start.1 = ((bf16[8,48,512]{2,1,0:T(8,128)(2,1)}), bf16[8,48,512]{2,1,0:T(8,128)(2,1)S(1)}, u32[]{:S(2)}, u32[]{:S(2)}) async-start(bf16[8,48,512]{2,1,0:T(8,128)(2,1)} %reduce-scatter.2.cloned.1.call-done), calls=%async_computation.2 | async-start | bytes 786432 | tf_op jit(solution)/shard_map/all_to_all | solution.py:185
  175.9 11.4 %all-to-all-done.1 = bf16[8,48,512]{2,1,0:T(8,128)(2,1)S(1)} async-done(((bf16[8,48,512]{2,1,0:T(8,128)(2,1)}), bf16[8,48,512]{2,1,0:T(8,128)(2,1)S(1)}, u32[]{:S(2)}, u32[]{:S(2)}) %all-to-all-start.1) | async-done | bytes 393248 | tf_op jit(solution)/shard_map/all_to_all | solution.py:185
  187.3 1.2 gather_fusion.1
  (70 shorter events, 8.8 us)
Async XLA Ops:
  6.5 133.4 %copy-start = (bf16[1,512,2048]{2,1,0:T(8,128)(2,1)S(1)}, bf16[1,512,2048]{2,1,0:T(8,128)(2,1)}, u32[]{:S(2)}) copy-start(bf16[1,512,2048]{2,1,0:T(8,128)(2,1)} %param.27) | copy-start | bytes 6291460
  6.5 88.0 %all-gather.6.cloned.1.call-start = ((), (), s32[]{:S(2)}) async-start(), calls=%async_computation.5 | async-start | bytes 2621440 | tf_op jit(solution)/shard_map/all_gather | solution.py:140
  41.0 1.4 copy-start.1
  43.8 29.1 %copy-start.2 = (bf16[512,2048]{1,0:T(8,128)(2,1)S(1)}, bf16[512,2048]{1,0:T(8,128)(2,1)}, u32[]{:S(2)}) copy-start(bf16[512,2048]{1,0:T(8,128)(2,1)} %param.21) | copy-start | bytes 6291460
  72.9 1.4 copy-start.4
  74.2 61.5 %all-gather.4.cloned.1.call-start = ((), (), s32[]{:S(2)}) async-start(), calls=%async_computation.3 | async-start | bytes 1966080 | tf_op jit(solution)/shard_map/all_gather | solution.py:174
  118.1 52.1 %reduce-scatter.2.cloned.1.call-start = ((), (), s32[]{:S(2)}) async-start(), calls=%async_computation.4 | async-start | bytes 1966080 | tf_op jit(solution)/shard_map/reduce_scatter | solution.py:182
  135.7 3.2 %copy-start.5 = (bf16[1,2048,512]{2,1,0:T(8,128)(2,1)S(1)}, bf16[1,2048,512]{2,1,0:T(8,128)(2,1)}, u32[]{:S(2)}) copy-start(bf16[1,2048,512]{2,1,0:T(8,128)(2,1)} %param.26) | copy-start | bytes 6291460
  135.7 3.2 %copy-start.6 = (bf16[8,48,2048]{2,1,0:T(8,128)(2,1)S(1)}, bf16[8,48,2048]{2,1,0:T(8,128)(2,1)}, u32[]{:S(2)}) copy-start(bf16[8,48,2048]{2,1,0:T(8,128)(2,1)} %all-gather.4.cloned.1.call-done) | copy-start | bytes 4718596
  142.1 33.7 %copy-start.3 = (f32[128,2]{0,1:T(2,128)S(1)}, f32[128,2]{0,1:T(2,128)}, u32[]{:S(2)}) copy-start(f32[128,2]{0,1:T(2,128)} %param.23) | copy-start | bytes 3076
  170.2 17.1 %all-to-all-start.1 = ((bf16[8,48,512]{2,1,0:T(8,128)(2,1)}), bf16[8,48,512]{2,1,0:T(8,128)(2,1)S(1)}, u32[]{:S(2)}, u32[]{:S(2)}) async-start(bf16[8,48,512]{2,1,0:T(8,128)(2,1)} %reduce-scatter.2.cloned.1.call-done), calls=%async_computation.2 | async-start | bytes 786432 | tf_op jit(solution)/shard_map/all_to_all | solution.py:185
Sparse Core Ops, SparseCore 0:
  74.3 20.1 all-gather.5
  118.3 17.3 all-gather.3
  142.2 27.9 reduce-scatter.1
